TPU v7x, 32 devices: a whole 2x2x4 slice. The times are simulated.
32 devices in a mesh: row: 4 (over y, x), col: 8 (over z, core).
Axes of the slice: x: 2, y: 2, z: 4, core: 2. Of those that a mesh axis runs over, the one named last changes fastest.
Arguments:
- mix_input: bfloat16 [4, 4096, 512], P(None, ('row', 'col')), may hold values from -6 to 6
- group_maps: bfloat16 [4, 128, 128], replicated, may hold values from -0.5 to 0.5
- out_map: bfloat16 [512, 2048], replicated, may hold values from -0.25 to 0.25
Outputs:
- mixed: bfloat16 [4, 4096, 2048], P(None, ('row', 'col'))
All inputs are finite; a program needn't handle non-finite values.
Results may differ from a plain program's by a relative error of at most 0.011.
Values may be sent and summed in bfloat16 or wider, within the bound.
A program may use at most 64 MiB of HBM per device.

v0:
```python
import math
import jax
import jax.numpy as jnp
from jax import lax
from jax.sharding import PartitionSpec as P

precise = lax.Precision.HIGHEST


def angle_pair(left_ids, right_ids, modulus):
    turn_count = left_ids[:, None] * right_ids[None, :] % modulus
    angles = turn_count.astype(jnp.float32) * (2.0 * math.pi / modulus)
    return (jnp.cos(angles), jnp.sin(angles))


def rotate(real_part, imag_part, cosine, sine_part):
    return (real_part * cosine + imag_part * sine_part, imag_part * cosine - real_part * sine_part)


def transform(real_in, imag_in, cosine, sine_part, einsum_form):
    real_out = jnp.einsum(einsum_form, real_in, cosine, precision=precise) + jnp.einsum(
        einsum_form, imag_in, sine_part, precision=precise
    )
    imag_out = jnp.einsum(einsum_form, imag_in, cosine, precision=precise) - jnp.einsum(
        einsum_form, real_in, sine_part, precision=precise
    )
    return (real_out, imag_out)


def per_device(mix_input, group_maps, out_map):
    sequences, positions, channels = mix_input.shape
    group_count, group_width, _ = group_maps.shape
    row_count = lax.axis_size("row")
    col_count = lax.axis_size("col")
    row_id = lax.axis_index("row")
    col_id = lax.axis_index("col")
    block_span = col_count * positions
    length = row_count * block_span
    norm_factor = 1.0 / math.sqrt(length * group_width)
    width_ids = jnp.arange(group_width, dtype=jnp.int32)
    real_tab, sine_tab = angle_pair(width_ids, width_ids, group_width)
    imag_tab = -sine_tab
    lane_count = real_tab.shape[1]
    signal = mix_input.astype(jnp.float32).reshape(sequences, positions, group_count, group_width)
    real_part = jnp.einsum("spgj,jl->sglp", signal, real_tab, precision=precise)
    imag_part = jnp.einsum("spgj,jl->sglp", signal, imag_tab, precision=precise)
    total_items = sequences * group_count * lane_count
    row_items = total_items // row_count
    dev_items = row_items // col_count
    send_shape = (row_count, row_items, 1, positions)
    col_shape = (col_count, dev_items, row_count, 1, positions)
    row_ids = jnp.arange(row_count, dtype=jnp.int32)
    pos_ids = jnp.arange(positions, dtype=jnp.int32)
    col_ids = jnp.arange(col_count, dtype=jnp.int32)
    row_cos, row_sin = angle_pair(row_ids, row_ids, row_count)
    turn_cos, turn_sin = angle_pair(row_ids, col_id * positions + pos_ids, length)
    col_cos, col_sin = angle_pair(col_ids, col_ids, col_count)
    step_cos, step_sin = angle_pair(col_ids, pos_ids, block_span)
    pos_cos, pos_sin = angle_pair(pos_ids, pos_ids, positions)
    row_send = (real_part.reshape(send_shape), imag_part.reshape(send_shape))
    pieces = (
        lax.all_to_all(row_send[0], "row", split_axis=0, concat_axis=2, tiled=True),
        lax.all_to_all(row_send[1], "row", split_axis=0, concat_axis=2, tiled=True),
    )
    spun_pair = transform(pieces[0][0], pieces[1][0], row_cos, row_sin, "nrp,rk->nkp")
    real_out, imag_out = rotate(spun_pair[0], spun_pair[1], turn_cos, turn_sin)
    real_rows = real_out[None]
    imag_rows = imag_out[None]
    pieces = (
        lax.all_to_all(
            real_rows.reshape(col_shape), "col", split_axis=0, concat_axis=3, tiled=True
        ),
        lax.all_to_all(
            imag_rows.reshape(col_shape), "col", split_axis=0, concat_axis=3, tiled=True
        ),
    )
    spun_pair = transform(pieces[0][0], pieces[1][0], col_cos, col_sin, "nacp,cb->nabp")
    turned = rotate(spun_pair[0], spun_pair[1], step_cos, step_sin)
    real_out = jnp.einsum("nabp,pq->nqba", turned[0], pos_cos, precision=precise) + jnp.einsum(
        "nabp,pq->nqba", turned[1], pos_sin, precision=precise
    )
    real_spec = real_out.reshape(1, real_out.shape[0], length)
    spectrum = real_spec[0][:, None]
    spectrum = (spectrum * norm_factor).astype(jnp.bfloat16)
    halves = spectrum.shape[1]
    spectrum = spectrum.reshape(1, dev_items, halves, row_count, col_count, positions)
    returned = lax.all_to_all(spectrum, "col", split_axis=4, concat_axis=0, tiled=True)
    held_groups = sequences * group_count // row_count
    returned = returned.reshape(held_groups, lane_count, halves, row_count, positions)
    full_width = returned[:, :, 0]
    group_ids = (row_id * held_groups + jnp.arange(held_groups, dtype=jnp.int32)) % group_count
    picker = (group_ids[:, None] == jnp.arange(group_count, dtype=jnp.int32)[None, :]).astype(
        jnp.bfloat16
    )
    chosen = jnp.einsum(
        "hg,glm->hlm", picker, group_maps, preferred_element_type=jnp.float32
    ).astype(jnp.bfloat16)
    grouped = jnp.einsum(
        "hlap,hlm->hapm", full_width, chosen, preferred_element_type=jnp.float32
    ).astype(jnp.bfloat16)
    grouped = grouped.reshape(1, held_groups, row_count, positions, group_width)
    arrived = lax.all_to_all(grouped, "row", split_axis=2, concat_axis=0, tiled=True)
    arrived = arrived.reshape(sequences, group_count, positions, group_width)
    mixed_out = jnp.einsum(
        "sgpm,gmn->spn",
        arrived,
        out_map.reshape(group_count, group_width, out_map.shape[1]),
        preferred_element_type=jnp.float32,
    )
    return mixed_out.astype(jnp.bfloat16)


def solution(mesh):
    return jax.shard_map(
        per_device,
        mesh=mesh,
        in_specs=(P(None, ("row", "col"), None), P(), P()),
        out_specs=P(None, ("row", "col"), None),
        check_vma=False,
    )
```

profile of v0, /device:TPU:0, one launch (start us, length us, event | category | flops | bytes accessed | tf_op | source)
XLA Modules:
  0.0 157.9 jit_solution(9652048484400523859)
XLA Ops:
  0.0 0.0 copy-start
  0.0 3.0 %fusion.30 = f32[128,4,128,4]{2,0,3,1:T(8,128)} fusion(bf16[4,128,512]{2,1,0:T(8,128)(2,1)} %param.3), kind=kOutput, calls=%fused_computation.42 | convolution fusion | flops 402882560 | bytes 1572864 | tf_op jit(solution)/shard_map/spgj,jl->sglp/dot_general | solution.py:45
  3.0 5.2 %all-to-all-start = ((f32[4,512,1,128]{3,1,2,0:T(8,128)}), f32[4,512,1,128]{3,1,2,0:T(8,128)S(1)}, u32[]{:S(2)}, u32[]{:S(2)}) async-start(f32[4,512,1,128]{3,1,2,0:T(8,128)} %bitcast.153), calls=%async_computation | async-start | bytes 2097152 | tf_op jit(solution)/shard_map/all_to_all | solution.py:62
  8.2 2.9 %fusion.28 = f32[128,4,128,4]{2,0,3,1:T(8,128)} fusion(bf16[4,128,512]{2,1,0:T(8,128)(2,1)} %param.3), kind=kOutput, calls=%fused_computation.40 | convolution fusion | flops 402898944 | bytes 1572864 | tf_op jit(solution)/shard_map/spgj,jl->sglp/dot_general | solution.py:46
  11.1 10.7 %all-to-all-done = f32[4,512,1,128]{3,1,2,0:T(8,128)S(1)} async-done(((f32[4,512,1,128]{3,1,2,0:T(8,128)}), f32[4,512,1,128]{3,1,2,0:T(8,128)S(1)}, u32[]{:S(2)}, u32[]{:S(2)}) %all-to-all-start) | async-done | bytes 1048608 | tf_op jit(solution)/shard_map/all_to_all | solution.py:62
  21.8 1.0 copy-done.1
  22.8 3.5 %all-to-all-start.1 = ((f32[4,512,1,128]{3,1,2,0:T(8,128)}), f32[4,512,1,128]{3,1,2,0:T(8,128)S(1)}, u32[]{:S(2)}, u32[]{:S(2)}) async-start(f32[4,512,1,128]{3,1,2,0:T(8,128)} %bitcast.152), calls=%async_computation.1 | async-start | bytes 2097152 | tf_op jit(solution)/shard_map/all_to_all | solution.py:63
  26.3 0.1 fusion.94
  26.4 4.6 %fusion.12 = f32[4,512,128]{2,0,1:T(4,128)} fusion(f32[4,512,1,128]{3,1,2,0:T(8,128)} %copy-done.1), kind=kOutput, calls=%fused_computation.20 | convolution fusion | flops 12583136 | bytes 2097152 | tf_op jit(solution)/shard_map/nrp,rk->nkp/dot_general | solution.py:21
  31.0 8.5 %all-to-all-done.1 = f32[4,512,1,128]{3,1,2,0:T(8,128)S(1)} async-done(((f32[4,512,1,128]{3,1,2,0:T(8,128)}), f32[4,512,1,128]{3,1,2,0:T(8,128)S(1)}, u32[]{:S(2)}, u32[]{:S(2)}) %all-to-all-start.1) | async-done | bytes 1048608 | tf_op jit(solution)/shard_map/all_to_all | solution.py:63
  39.5 2.4 %fusion.14 = f32[4,512,128]{2,0,1:T(4,128)S(1)} fusion(f32[4,512,1,128]{3,1,2,0:T(8,128)S(1)} %all-to-all-done.1), kind=kOutput, calls=%fused_computation.22 | convolution fusion | flops 12583136 | bytes 2097152 | tf_op jit(solution)/shard_map/nrp,rk->nkp/dot_general | solution.py:24
  41.8 0.0 copy-start.2
  41.8 2.5 %convolution_add_fusion.2 = f32[4,512,128]{2,0,1:T(4,128)S(1)} fusion(f32[4,512,128]{2,0,1:T(4,128)S(1)} %copy-done.3, f32[4,512,1,128]{3,1,2,0:T(8,128)S(1)} %all-to-all-done.1), kind=kOutput, calls=%fused_computation.6 | convolution fusion | flops 12845280 | bytes 3145728 | tf_op jit(solution)/shard_map/nrp,rk->nkp/dot_general | solution.py:21
  44.4 3.9 %multiply_add_fusion = (f32[4,512,128]{2,0,1:T(4,128)}, f32[4,512,128]{2,0,1:T(4,128)S(1)}) fusion(f32[4,512,128]{2,0,1:T(4,128)S(1)} %convolution_add_fusion.2, f32[4,128]{1,0:T(4,128)S(1)} %get-tuple-element.10, f32[4,128]{1,0:T(4,128)S(1)} %get-tuple-element.9, f32[4,512,128]{2,0,1:T(4,128)S(1)} %fusion.14, f32[4,512,1,128]{3,1,2,0:T(8,128)S(1)} %copy-done.2), kind=kOutput, calls=%fused_computation.31 | convolution fusion | flops 14418144 | bytes 5246976 | tf_op jit(solution)/shard_map/nrp,rk->nkp/dot_general | solution.py:24
  48.3 31.3 %all_to_all.90 = f32[8,64,4,1,128]{4,2,1,3,0:T(4,128)S(1)} all-to-all(f32[8,64,4,1,128]{4,2,1,3,0:T(4,128)S(1)} %bitcast.155), channel_id=1, replica_groups=mesh['row'=4,'col'=8] {'col'}, dimensions={0} | all-to-all | bytes 2097152 | tf_op jit(solution)/shard_map/all_to_all | solution.py:73
  79.5 4.4 %all-to-all-start.2 = ((f32[8,64,4,1,128]{4,2,1,3,0:T(4,128)}), f32[8,64,4,1,128]{4,2,1,3,0:T(4,128)}, u32[]{:S(2)}, u32[]{:S(2)}) async-start(f32[8,64,4,1,128]{4,2,1,3,0:T(4,128)} %bitcast.154), calls=%async_computation.2 | async-start | bytes 2097152 | tf_op jit(solution)/shard_map/all_to_all | solution.py:70
  84.0 0.1 fusion.82
  84.0 2.5 %fusion.8 = f32[8,64,4,128]{3,0,2,1:T(8,128)} fusion(f32[8,64,4,1,128]{4,2,1,3,0:T(4,128)S(1)} %all_to_all.90), kind=kOutput, calls=%fused_computation.16 | convolution fusion | flops 25166720 | bytes 2097152 | tf_op jit(solution)/shard_map/nacp,cb->nabp/dot_general | solution.py:24
  86.5 23.8 %all-to-all-done.2 = f32[8,64,4,1,128]{4,2,1,3,0:T(4,128)} async-done(((f32[8,64,4,1,128]{4,2,1,3,0:T(4,128)}), f32[8,64,4,1,128]{4,2,1,3,0:T(4,128)}, u32[]{:S(2)}, u32[]{:S(2)}) %all-to-all-start.2) | async-done | bytes 1048608 | tf_op jit(solution)/shard_map/all_to_all | solution.py:70
  110.4 2.8 %fusion.6 = f32[8,64,4,128]{3,0,2,1:T(8,128)S(1)} fusion(f32[8,64,4,1,128]{4,2,1,3,0:T(4,128)} %all-to-all-done.2), kind=kOutput, calls=%fused_computation.14 | convolution fusion | flops 25166720 | bytes 2097152 | tf_op jit(solution)/shard_map/nacp,cb->nabp/dot_general | solution.py:21
  113.2 2.7 %convolution_subtract_fusion = f32[8,64,4,128]{3,0,2,1:T(8,128)S(1)} fusion(f32[8,64,4,128]{3,0,2,1:T(8,128)S(1)} %copy-done.4, f32[8,64,4,1,128]{4,2,1,3,0:T(4,128)} %all-to-all-done.2), kind=kOutput, calls=%fused_computation.3 | convolution fusion | flops 25428864 | bytes 3145728 | tf_op jit(solution)/shard_map/nacp,cb->nabp/dot_general | solution.py:24
  115.9 1.7 %subtract_bitcast_fusion = (f32[64,4,8,128]{3,2,1,0:T(8,128)S(1)}, f32[64,4,8,128]{3,2,1,0:T(8,128)S(1)}) fusion(f32[8,64,4,128]{3,0,2,1:T(8,128)S(1)} %convolution_subtract_fusion, f32[8,128]{1,0:T(8,128)S(1)} %get-tuple-element.11, f32[8,128]{1,0:T(8,128)S(1)} %get-tuple-element.12, f32[8,64,4,128]{3,0,2,1:T(8,128)S(1)} %fusion.6, ...), kind=kOutput, calls=%fused_computation.28 | convolution fusion | flops 27001728 | bytes 5251072 | tf_op jit(solution)/shard_map/nacp,cb->nabp/dot_general | solution.py:21
  117.7 1.9 %fusion.18 = f32[128,64,4,8]{0,1,3,2:T(8,128)S(1)} fusion(f32[64,4,8,128]{3,2,1,0:T(8,128)S(1)} %get-tuple-element.6), kind=kOutput, calls=%fused_computation.26 | convolution fusion | flops 402882560 | bytes 2097152 | tf_op jit(solution)/shard_map/nabp,pq->nqba/dot_general | solution.py:79
  119.5 2.7 %fusion.3 = bf16[64,128,8,4]{1,0,2,3:T(8,128)(2,1)} fusion(f32[128,64,4,8]{0,1,3,2:T(8,128)S(1)} %fusion.18, f32[64,4,8,128]{3,2,1,0:T(8,128)S(1)} %get-tuple-element.5), kind=kOutput, calls=%fused_computation.10 | convolution fusion | flops 403668992 | bytes 2621440 | tf_op jit(solution)/shard_map/nabp,pq->nqba/dot_general | solution.py:79
  122.2 1.9 %copy.43 = bf16[64,128,8,4]{0,3,2,1:T(4,128)(2,1)S(1)} copy(bf16[64,128,8,4]{1,0,2,3:T(8,128)(2,1)} %fusion.3) | data formatting | bytes 1048576 | tf_op jit(solution)/shard_map/convert_element_type | solution.py:84
  124.1 1.1 copy.44
  125.2 3.5 %all-to-all-start.4 = ((bf16[1,64,1,4,8,128]{5,1,3,2,0,4:T(8,128)(2,1)}), bf16[1,64,1,4,8,128]{5,1,3,2,0,4:T(8,128)(2,1)S(1)}, u32[]{:S(2)}, u32[]{:S(2)}) async-start(bf16[1,64,1,4,8,128]{5,1,3,2,0,4:T(8,128)(2,1)} %copy.44), calls=%async_computation.4 | async-start | bytes 1048576 | tf_op jit(solution)/shard_map/all_to_all | solution.py:87
  128.7 0.3 fusion.4
  129.0 14.9 %all-to-all-done.4 = bf16[1,64,1,4,8,128]{5,1,3,2,0,4:T(8,128)(2,1)S(1)} async-done(((bf16[1,64,1,4,8,128]{5,1,3,2,0,4:T(8,128)(2,1)}), bf16[1,64,1,4,8,128]{5,1,3,2,0,4:T(8,128)(2,1)S(1)}, u32[]{:S(2)}, u32[]{:S(2)}) %all-to-all-start.4) | async-done | bytes 524320 | tf_op jit(solution)/shard_map/all_to_all | solution.py:87
  144.0 0.4 fusion.2
  144.4 10.9 %all_to_all.91 = bf16[1,4,4,128,128]{4,3,1,0,2:T(8,128)(2,1)S(1)} all-to-all(bf16[1,4,4,128,128]{4,3,1,0,2:T(8,128)(2,1)S(1)} %copy.49), channel_id=1, replica_groups=mesh['row'=4,'col'=8] {'row'}, dimensions={2} | all-to-all | bytes 1048576 | tf_op jit(solution)/shard_map/all_to_all | solution.py:102
  155.3 2.6 %bitcast_convert_fusion = bf16[4,128,2048]{2,1,0:T(8,128)(2,1)} fusion(bf16[4,128,2048,1]{2,1,3,0:T(8,128)(2,1)S(1)} %bitcast.150, bf16[1,4,4,128,128]{4,3,1,0,2:T(8,128)(2,1)S(1)} %all_to_all.91), kind=kOutput, calls=%fused_computation | convolution fusion | flops 1074790400 | bytes 4718592 | tf_op jit(solution)/shard_map/sgpm,gmn->spn/dot_general | solution.py:104
  (13 shorter events, 0.1 us)
Async XLA Ops:
  0.0 155.3 %copy-start = (bf16[512,2048]{1,0:T(8,128)(2,1)S(1)}, bf16[512,2048]{1,0:T(8,128)(2,1)}, u32[]{:S(2)}) copy-start(bf16[512,2048]{1,0:T(8,128)(2,1)} %param.5) | copy-start | bytes 6291460
  3.0 18.8 %all-to-all-start = ((f32[4,512,1,128]{3,1,2,0:T(8,128)}), f32[4,512,1,128]{3,1,2,0:T(8,128)S(1)}, u32[]{:S(2)}, u32[]{:S(2)}) async-start(f32[4,512,1,128]{3,1,2,0:T(8,128)} %bitcast.153), calls=%async_computation | async-start | bytes 2097152 | tf_op jit(solution)/shard_map/all_to_all | solution.py:62
  21.8 1.0 copy-start.1
  22.8 16.6 %all-to-all-start.1 = ((f32[4,512,1,128]{3,1,2,0:T(8,128)}), f32[4,512,1,128]{3,1,2,0:T(8,128)S(1)}, u32[]{:S(2)}, u32[]{:S(2)}) async-start(f32[4,512,1,128]{3,1,2,0:T(8,128)} %bitcast.152), calls=%async_computation.1 | async-start | bytes 2097152 | tf_op jit(solution)/shard_map/all_to_all | solution.py:63
  39.5 2.4 %copy-start.3 = (f32[4,512,128]{2,0,1:T(4,128)S(1)}, f32[4,512,128]{2,0,1:T(4,128)}, u32[]{:S(2)}) copy-start(f32[4,512,128]{2,0,1:T(4,128)} %fusion.12) | copy-start | bytes 3145732
  41.8 2.5 %copy-start.2 = (f32[4,512,1,128]{3,1,2,0:T(8,128)S(1)}, f32[4,512,1,128]{3,1,2,0:T(8,128)}, u32[]{:S(2)}) copy-start(f32[4,512,1,128]{3,1,2,0:T(8,128)} %copy-done.1) | copy-start | bytes 3145732
  79.5 30.8 %all-to-all-start.2 = ((f32[8,64,4,1,128]{4,2,1,3,0:T(4,128)}), f32[8,64,4,1,128]{4,2,1,3,0:T(4,128)}, u32[]{:S(2)}, u32[]{:S(2)}) async-start(f32[8,64,4,1,128]{4,2,1,3,0:T(4,128)} %bitcast.154), calls=%async_computation.2 | async-start | bytes 2097152 | tf_op jit(solution)/shard_map/all_to_all | solution.py:70
  110.4 2.8 %copy-start.4 = (f32[8,64,4,128]{3,0,2,1:T(8,128)S(1)}, f32[8,64,4,128]{3,0,2,1:T(8,128)}, u32[]{:S(2)}) copy-start(f32[8,64,4,128]{3,0,2,1:T(8,128)} %fusion.8) | copy-start | bytes 3145732
  122.2 6.5 %copy-start.5 = (bf16[4,128,128]{2,1,0:T(8,128)(2,1)S(1)}, bf16[4,128,128]{2,1,0:T(8,128)(2,1)}, u32[]{:S(2)}) copy-start(bf16[4,128,128]{2,1,0:T(8,128)(2,1)} %param.4) | copy-start | bytes 393220
  125.2 18.8 %all-to-all-start.4 = ((bf16[1,64,1,4,8,128]{5,1,3,2,0,4:T(8,128)(2,1)}), bf16[1,64,1,4,8,128]{5,1,3,2,0,4:T(8,128)(2,1)S(1)}, u32[]{:S(2)}, u32[]{:S(2)}) async-start(bf16[1,64,1,4,8,128]{5,1,3,2,0,4:T(8,128)(2,1)} %copy.44), calls=%async_computation.4 | async-start | bytes 1048576 | tf_op jit(solution)/shard_map/all_to_all | solution.py:87
where the time goes:
time: 159 us; the launch traced here: 158 us
  waiting for transfers between devices  58 us (36%)
  blocking collectives  42.2 us (27%)
  matrix products  36.8 us (23%)
  starting transfers between devices  16.6 us (10%)
  local copies, waits for them, and re-layouts  4.07 us (3%)
    all_to_all x1, blocking collectives, per_device(): lax.all_to_all(imag_rows.reshape(col_shape), 'col', split_axis=0, concat_...  31.3 us
    all_to_all x1, waiting for transfers between devices, per_device(): lax.all_to_all(real_rows.reshape(col_shape), 'col', split_axis=0, concat_...  23.8 us
    all_to_all x1, waiting for transfers between devices, per_device(): lax.all_to_all(spectrum, 'col', split_axis=4, concat_axis=0, tiled=True)  14.9 us
    all_to_all x1, blocking collectives, per_device(): lax.all_to_all(grouped, 'row', split_axis=2, concat_axis=0, tiled=True)  10.9 us
    all_to_all x1, waiting for transfers between devices, per_device(): lax.all_to_all(row_send[0], 'row', split_axis=0, concat_axis=2, tiled=True)  10.7 us
    all_to_all x1, waiting for transfers between devices, per_device(): lax.all_to_all(row_send[1], 'row', split_axis=0, concat_axis=2, tiled=True)  8.48 us
    dot_general x2, matrix products, transform(): jnp.einsum(einsum_form, real_in, cosine, precision=precise)  7.38 us
    dot_general x2, matrix products, transform(): jnp.einsum(einsum_form, real_in, sine_part, precision=precise)  6.61 us
  transfers between devices with their start and end apart: 4, of which 4 were waited for; matrix products, arithmetic and copies ran while one was open for 7% of the time, Pallas kernels for 0%

commit v1 on v0

--- a/solution.py
+++ b/solution.py
@@ -84,7 +84,11 @@
     spectrum = (spectrum * norm_factor).astype(jnp.bfloat16)
     halves = spectrum.shape[1]
     spectrum = spectrum.reshape(1, dev_items, halves, row_count, col_count, positions)
-    returned = lax.all_to_all(spectrum, "col", split_axis=4, concat_axis=0, tiled=True)
+    g_now = lax.axis_size("col")
+    opened = jnp.split(spectrum, g_now, axis=4)
+    high = jnp.stack(opened, axis=0)
+    extra = lax.all_to_all(high, "col", 0, 0)
+    returned = jnp.concatenate(extra, axis=0)
     held_groups = sequences * group_count // row_count
     returned = returned.reshape(held_groups, lane_count, halves, row_count, positions)
     full_width = returned[:, :, 0]

time: 159 us -> 165 us (1.038)
  local copies, waits for them, and re-layouts: 4.07 us -> 10.6 us
    unnamed x12 -> x19, local copies, waits for them, and re-layouts: 0.99 us -> 5.64 us
    another operation x0 -> x2, local copies, waits for them, and re-layouts: none -> 3 us  [per_device(): high = jnp.stack(opened, axis=0)]
  transfers between devices with their start and end apart: 4 -> 4, of which waited for: 4 -> 4; matrix products, arithmetic and copies ran while one was open for 7% -> 6% of each run, Pallas kernels for 0% -> 0%
where the time goes in v1:
time: 165 us; the launch traced here: 164 us
  waiting for transfers between devices  58 us (35%)
  blocking collectives  42.2 us (26%)
  matrix products  36.8 us (22%)
  starting transfers between devices  16.6 us (10%)
  local copies, waits for them, and re-layouts  10.6 us (6%)
    all_to_all x1, blocking collectives, per_device(): lax.all_to_all(imag_rows.reshape(col_shape), 'col', split_axis=0, concat_...  31.3 us
    all_to_all x1, waiting for transfers between devices, per_device(): lax.all_to_all(real_rows.reshape(col_shape), 'col', split_axis=0, concat_...  23.8 us
    all_to_all x1, waiting for transfers between devices, per_device(): extra = lax.all_to_all(high, 'col', 0, 0)  14.9 us
    all_to_all x1, blocking collectives, per_device(): lax.all_to_all(grouped, 'row', split_axis=2, concat_axis=0, tiled=True)  10.9 us
    all_to_all x1, waiting for transfers between devices, per_device(): lax.all_to_all(row_send[0], 'row', split_axis=0, concat_axis=2, tiled=True)  10.7 us
    all_to_all x1, waiting for transfers between devices, per_device(): lax.all_to_all(row_send[1], 'row', split_axis=0, concat_axis=2, tiled=True)  8.48 us
    dot_general x2, matrix products, transform(): jnp.einsum(einsum_form, real_in, cosine, precision=precise)  7.38 us
    dot_general x2, matrix products, transform(): jnp.einsum(einsum_form, real_in, sine_part, precision=precise)  6.61 us
  transfers between devices with their start and end apart: 4, of which 4 were waited for; matrix products, arithmetic and copies ran while one was open for 6% of the time, Pallas kernels for 0%

profile of v1, /device:TPU:0, one launch (start us, length us, event | category | flops | bytes accessed | tf_op | source)
XLA Modules:
  0.0 164.4 jit_solution(14262760907626819341)
XLA Ops:
  0.0 3.0 %fusion.30 = f32[128,4,128,4]{2,0,3,1:T(8,128)} fusion(bf16[4,128,512]{2,1,0:T(8,128)(2,1)} %param.3), kind=kOutput, calls=%fused_computation.42 | convolution fusion | flops 402882560 | bytes 1572864 | tf_op jit(solution)/shard_map/spgj,jl->sglp/dot_general | solution.py:45
  3.0 5.2 %all-to-all-start = ((f32[4,512,1,128]{3,1,2,0:T(8,128)}), f32[4,512,1,128]{3,1,2,0:T(8,128)S(1)}, u32[]{:S(2)}, u32[]{:S(2)}) async-start(f32[4,512,1,128]{3,1,2,0:T(8,128)} %bitcast.200), calls=%async_computation | async-start | bytes 2097152 | tf_op jit(solution)/shard_map/all_to_all | solution.py:62
  8.2 2.9 %fusion.28 = f32[128,4,128,4]{2,0,3,1:T(8,128)} fusion(bf16[4,128,512]{2,1,0:T(8,128)(2,1)} %param.3), kind=kOutput, calls=%fused_computation.40 | convolution fusion | flops 402898944 | bytes 1572864 | tf_op jit(solution)/shard_map/spgj,jl->sglp/dot_general | solution.py:46
  11.1 10.7 %all-to-all-done = f32[4,512,1,128]{3,1,2,0:T(8,128)S(1)} async-done(((f32[4,512,1,128]{3,1,2,0:T(8,128)}), f32[4,512,1,128]{3,1,2,0:T(8,128)S(1)}, u32[]{:S(2)}, u32[]{:S(2)}) %all-to-all-start) | async-done | bytes 1048608 | tf_op jit(solution)/shard_map/all_to_all | solution.py:62
  21.8 1.0 copy-done.1
  22.8 3.5 %all-to-all-start.1 = ((f32[4,512,1,128]{3,1,2,0:T(8,128)}), f32[4,512,1,128]{3,1,2,0:T(8,128)S(1)}, u32[]{:S(2)}, u32[]{:S(2)}) async-start(f32[4,512,1,128]{3,1,2,0:T(8,128)} %bitcast.199), calls=%async_computation.1 | async-start | bytes 2097152 | tf_op jit(solution)/shard_map/all_to_all | solution.py:63
  26.4 4.6 %fusion.12 = f32[4,512,128]{2,0,1:T(4,128)} fusion(f32[4,512,1,128]{3,1,2,0:T(8,128)} %copy-done.1), kind=kOutput, calls=%fused_computation.20 | convolution fusion | flops 12583136 | bytes 2097152 | tf_op jit(solution)/shard_map/nrp,rk->nkp/dot_general | solution.py:21
  31.0 8.5 %all-to-all-done.1 = f32[4,512,1,128]{3,1,2,0:T(8,128)S(1)} async-done(((f32[4,512,1,128]{3,1,2,0:T(8,128)}), f32[4,512,1,128]{3,1,2,0:T(8,128)S(1)}, u32[]{:S(2)}, u32[]{:S(2)}) %all-to-all-start.1) | async-done | bytes 1048608 | tf_op jit(solution)/shard_map/all_to_all | solution.py:63
  39.5 2.4 %fusion.14 = f32[4,512,128]{2,0,1:T(4,128)S(1)} fusion(f32[4,512,1,128]{3,1,2,0:T(8,128)S(1)} %all-to-all-done.1), kind=kOutput, calls=%fused_computation.22 | convolution fusion | flops 12583136 | bytes 2097152 | tf_op jit(solution)/shard_map/nrp,rk->nkp/dot_general | solution.py:24
  41.8 2.5 %convolution_add_fusion.2 = f32[4,512,128]{2,0,1:T(4,128)S(1)} fusion(f32[4,512,128]{2,0,1:T(4,128)S(1)} %copy-done.3, f32[4,512,1,128]{3,1,2,0:T(8,128)S(1)} %all-to-all-done.1), kind=kOutput, calls=%fused_computation.6 | convolution fusion | flops 12845280 | bytes 3145728 | tf_op jit(solution)/shard_map/nrp,rk->nkp/dot_general | solution.py:21
  44.4 3.9 %multiply_add_fusion = (f32[4,512,128]{2,0,1:T(4,128)}, f32[4,512,128]{2,0,1:T(4,128)S(1)}) fusion(f32[4,512,128]{2,0,1:T(4,128)S(1)} %convolution_add_fusion.2, f32[4,128]{1,0:T(4,128)S(1)} %get-tuple-element.10, f32[4,128]{1,0:T(4,128)S(1)} %get-tuple-element.9, f32[4,512,128]{2,0,1:T(4,128)S(1)} %fusion.14, f32[4,512,1,128]{3,1,2,0:T(8,128)S(1)} %copy-done.2), kind=kOutput, calls=%fused_computation.31 | convolution fusion | flops 14418144 | bytes 5246976 | tf_op jit(solution)/shard_map/nrp,rk->nkp/dot_general | solution.py:24
  48.3 31.3 %all_to_all.80 = f32[8,64,4,1,128]{4,2,1,3,0:T(4,128)S(1)} all-to-all(f32[8,64,4,1,128]{4,2,1,3,0:T(4,128)S(1)} %bitcast.202), channel_id=1, replica_groups=mesh['row'=4,'col'=8] {'col'}, dimensions={0} | all-to-all | bytes 2097152 | tf_op jit(solution)/shard_map/all_to_all | solution.py:73
  79.5 4.4 %all-to-all-start.2 = ((f32[8,64,4,1,128]{4,2,1,3,0:T(4,128)}), f32[8,64,4,1,128]{4,2,1,3,0:T(4,128)}, u32[]{:S(2)}, u32[]{:S(2)}) async-start(f32[8,64,4,1,128]{4,2,1,3,0:T(4,128)} %bitcast.201), calls=%async_computation.2 | async-start | bytes 2097152 | tf_op jit(solution)/shard_map/all_to_all | solution.py:70
  84.0 2.5 %fusion.8 = f32[8,64,4,128]{3,0,2,1:T(8,128)} fusion(f32[8,64,4,1,128]{4,2,1,3,0:T(4,128)S(1)} %all_to_all.80), kind=kOutput, calls=%fused_computation.16 | convolution fusion | flops 25166720 | bytes 2097152 | tf_op jit(solution)/shard_map/nacp,cb->nabp/dot_general | solution.py:24
  86.5 23.8 %all-to-all-done.2 = f32[8,64,4,1,128]{4,2,1,3,0:T(4,128)} async-done(((f32[8,64,4,1,128]{4,2,1,3,0:T(4,128)}), f32[8,64,4,1,128]{4,2,1,3,0:T(4,128)}, u32[]{:S(2)}, u32[]{:S(2)}) %all-to-all-start.2) | async-done | bytes 1048608 | tf_op jit(solution)/shard_map/all_to_all | solution.py:70
  110.4 2.8 %fusion.6 = f32[8,64,4,128]{3,0,2,1:T(8,128)S(1)} fusion(f32[8,64,4,1,128]{4,2,1,3,0:T(4,128)} %all-to-all-done.2), kind=kOutput, calls=%fused_computation.14 | convolution fusion | flops 25166720 | bytes 2097152 | tf_op jit(solution)/shard_map/nacp,cb->nabp/dot_general | solution.py:21
  113.2 2.7 %convolution_subtract_fusion = f32[8,64,4,128]{3,0,2,1:T(8,128)S(1)} fusion(f32[8,64,4,128]{3,0,2,1:T(8,128)S(1)} %copy-done.4, f32[8,64,4,1,128]{4,2,1,3,0:T(4,128)} %all-to-all-done.2), kind=kOutput, calls=%fused_computation.3 | convolution fusion | flops 25428864 | bytes 3145728 | tf_op jit(solution)/shard_map/nacp,cb->nabp/dot_general | solution.py:24
  115.9 1.7 %subtract_bitcast_fusion = (f32[64,4,8,128]{3,2,1,0:T(8,128)S(1)}, f32[64,4,8,128]{3,2,1,0:T(8,128)S(1)}) fusion(f32[8,64,4,128]{3,0,2,1:T(8,128)S(1)} %convolution_subtract_fusion, f32[8,128]{1,0:T(8,128)S(1)} %get-tuple-element.11, f32[8,128]{1,0:T(8,128)S(1)} %get-tuple-element.12, f32[8,64,4,128]{3,0,2,1:T(8,128)S(1)} %fusion.6, ...), kind=kOutput, calls=%fused_computation.28 | convolution fusion | flops 27001728 | bytes 5251072 | tf_op jit(solution)/shard_map/nacp,cb->nabp/dot_general | solution.py:21
  117.7 1.9 %fusion.18 = f32[128,64,4,8]{0,1,3,2:T(8,128)S(1)} fusion(f32[64,4,8,128]{3,2,1,0:T(8,128)S(1)} %get-tuple-element.6), kind=kOutput, calls=%fused_computation.26 | convolution fusion | flops 402882560 | bytes 2097152 | tf_op jit(solution)/shard_map/nabp,pq->nqba/dot_general | solution.py:79
  119.5 2.7 %fusion.3 = bf16[64,128,8,4]{1,0,2,3:T(8,128)(2,1)} fusion(f32[128,64,4,8]{0,1,3,2:T(8,128)S(1)} %fusion.18, f32[64,4,8,128]{3,2,1,0:T(8,128)S(1)} %get-tuple-element.5), kind=kOutput, calls=%fused_computation.10 | convolution fusion | flops 403668992 | bytes 2621440 | tf_op jit(solution)/shard_map/nabp,pq->nqba/dot_general | solution.py:79
  122.2 1.8 %copy.58 = bf16[64,128,8,4]{0,3,2,1:T(4,128)(2,1)S(1)} copy(bf16[64,128,8,4]{1,0,2,3:T(8,128)(2,1)} %fusion.3) | data formatting | bytes 1048576 | tf_op jit(solution)/shard_map/convert_element_type | solution.py:84
  124.0 0.7 fusion.44
  124.7 0.7 fusion.43
  125.4 0.7 fusion.42
  126.0 0.7 fusion.41
  127.4 0.7 fusion.39
  128.7 0.7 fusion.37
  129.4 2.3 %copy.67 = bf16[8,1,64,1,4,1,128]{6,2,5,4,3,1,0:T(8,128)(2,1)} copy(bf16[8,1,64,1,4,1,128]{2,6,4,5,3,1,0:T(8,128)(2,1)} %fusion.37) | data formatting | bytes 1048576 | tf_op jit(solution)/shard_map/stack | solution.py:89
  131.7 3.5 %all-to-all-start.4 = ((bf16[8,1,64,1,4,1,128]{6,2,5,4,3,1,0:T(8,128)(2,1)}), bf16[8,1,64,1,4,1,128]{6,2,5,4,3,1,0:T(8,128)(2,1)S(1)}, u32[]{:S(2)}, u32[]{:S(2)}) async-start(bf16[8,1,64,1,4,1,128]{6,2,5,4,3,1,0:T(8,128)(2,1)} %copy.67), calls=%async_computation.4 | async-start | bytes 1048576 | tf_op jit(solution)/shard_map/all_to_all | solution.py:90
  135.5 14.9 %all-to-all-done.4 = bf16[8,1,64,1,4,1,128]{6,2,5,4,3,1,0:T(8,128)(2,1)S(1)} async-done(((bf16[8,1,64,1,4,1,128]{6,2,5,4,3,1,0:T(8,128)(2,1)}), bf16[8,1,64,1,4,1,128]{6,2,5,4,3,1,0:T(8,128)(2,1)S(1)}, u32[]{:S(2)}, u32[]{:S(2)}) %all-to-all-start.4) | async-done | bytes 524320 | tf_op jit(solution)/shard_map/all_to_all | solution.py:90
  150.9 10.9 %all_to_all.81 = bf16[1,4,4,128,128]{4,3,1,0,2:T(8,128)(2,1)S(1)} all-to-all(bf16[1,4,4,128,128]{4,3,1,0,2:T(8,128)(2,1)S(1)} %copy.72), channel_id=1, replica_groups=mesh['row'=4,'col'=8] {'row'}, dimensions={2} | all-to-all | bytes 1048576 | tf_op jit(solution)/shard_map/all_to_all | solution.py:106
  161.8 2.6 %bitcast_convert_fusion = bf16[4,128,2048]{2,1,0:T(8,128)(2,1)} fusion(bf16[4,128,2048,1]{2,1,3,0:T(8,128)(2,1)S(1)} %bitcast.190, bf16[1,4,4,128,128]{4,3,1,0,2:T(8,128)(2,1)S(1)} %all_to_all.81), kind=kOutput, calls=%fused_computation | convolution fusion | flops 1074790400 | bytes 4718592 | tf_op jit(solution)/shard_map/sgpm,gmn->spn/dot_general | solution.py:108
  (21 shorter events, 2.2 us)
Async XLA Ops:
  0.0 161.8 %copy-start = (bf16[512,2048]{1,0:T(8,128)(2,1)S(1)}, bf16[512,2048]{1,0:T(8,128)(2,1)}, u32[]{:S(2)}) copy-start(bf16[512,2048]{1,0:T(8,128)(2,1)} %param.5) | copy-start | bytes 6291460
  3.0 18.8 %all-to-all-start = ((f32[4,512,1,128]{3,1,2,0:T(8,128)}), f32[4,512,1,128]{3,1,2,0:T(8,128)S(1)}, u32[]{:S(2)}, u32[]{:S(2)}) async-start(f32[4,512,1,128]{3,1,2,0:T(8,128)} %bitcast.200), calls=%async_computation | async-start | bytes 2097152 | tf_op jit(solution)/shard_map/all_to_all | solution.py:62
  21.8 1.0 copy-start.1
  22.8 16.6 %all-to-all-start.1 = ((f32[4,512,1,128]{3,1,2,0:T(8,128)}), f32[4,512,1,128]{3,1,2,0:T(8,128)S(1)}, u32[]{:S(2)}, u32[]{:S(2)}) async-start(f32[4,512,1,128]{3,1,2,0:T(8,128)} %bitcast.199), calls=%async_computation.1 | async-start | bytes 2097152 | tf_op jit(solution)/shard_map/all_to_all | solution.py:63
  39.5 2.4 %copy-start.3 = (f32[4,512,128]{2,0,1:T(4,128)S(1)}, f32[4,512,128]{2,0,1:T(4,128)}, u32[]{:S(2)}) copy-start(f32[4,512,128]{2,0,1:T(4,128)} %fusion.12) | copy-start | bytes 3145732
  41.8 2.5 %copy-start.2 = (f32[4,512,1,128]{3,1,2,0:T(8,128)S(1)}, f32[4,512,1,128]{3,1,2,0:T(8,128)}, u32[]{:S(2)}) copy-start(f32[4,512,1,128]{3,1,2,0:T(8,128)} %copy-done.1) | copy-start | bytes 3145732
  79.5 30.8 %all-to-all-start.2 = ((f32[8,64,4,1,128]{4,2,1,3,0:T(4,128)}), f32[8,64,4,1,128]{4,2,1,3,0:T(4,128)}, u32[]{:S(2)}, u32[]{:S(2)}) async-start(f32[8,64,4,1,128]{4,2,1,3,0:T(4,128)} %bitcast.201), calls=%async_computation.2 | async-start | bytes 2097152 | tf_op jit(solution)/shard_map/all_to_all | solution.py:70
  110.4 2.8 %copy-start.4 = (f32[8,64,4,128]{3,0,2,1:T(8,128)S(1)}, f32[8,64,4,128]{3,0,2,1:T(8,128)}, u32[]{:S(2)}) copy-start(f32[8,64,4,128]{3,0,2,1:T(8,128)} %fusion.8) | copy-start | bytes 3145732
  125.4 9.8 %copy-start.5 = (bf16[4,128,128]{2,1,0:T(8,128)(2,1)S(1)}, bf16[4,128,128]{2,1,0:T(8,128)(2,1)}, u32[]{:S(2)}) copy-start(bf16[4,128,128]{2,1,0:T(8,128)(2,1)} %param.4) | copy-start | bytes 393220
  131.7 18.8 %all-to-all-start.4 = ((bf16[8,1,64,1,4,1,128]{6,2,5,4,3,1,0:T(8,128)(2,1)}), bf16[8,1,64,1,4,1,128]{6,2,5,4,3,1,0:T(8,128)(2,1)S(1)}, u32[]{:S(2)}, u32[]{:S(2)}) async-start(bf16[8,1,64,1,4,1,128]{6,2,5,4,3,1,0:T(8,128)(2,1)} %copy.67), calls=%async_computation.4 | async-start | bytes 1048576 | tf_op jit(solution)/shard_map/all_to_all | solution.py:90
